TPU v7x, 32 devices: a whole 2x2x4 slice. The times are simulated.
32 devices in a mesh: sp: 4 (over y, x), tp: 8 (over z, core).
Axes of the slice: x: 2, y: 2, z: 4, core: 2. Of those that a mesh axis runs over, the one named last changes fastest.
Arguments:
- tokens: bfloat16 [8, 512, 4096], P('tp', 'sp'), may hold values from -6 to 6
- latent_down_matrix: bfloat16 [4096, 512], P('tp'), may hold values from -0.09375 to 0.09375
- rope_weight: bfloat16 [4096, 64], P('tp'), may hold values from -0.09375 to 0.09375
- latent_norm_scale: float32 [512], replicated, may hold values from 0.1 to 1.9
- key_up_matrix: bfloat16 [512, 32, 128], P(None, 'tp'), may hold values from -0.25 to 0.25
- value_up_matrix: bfloat16 [512, 32, 128], P(None, 'tp'), may hold values from -0.25 to 0.25
- query: bfloat16 [8, 32, 192], P('sp', 'tp'), may hold values from -126 to 126
Outputs:
- plain_key_cache: bfloat16 [8, 512, 32, 128], P('sp', None, 'tp')
- head_value_cache: bfloat16 [8, 512, 32, 128], P('sp', None, 'tp')
- rotated_key_cache: bfloat16 [8, 512, 64], P('sp')
- first_read: bfloat16 [8, 32, 128], P('sp', 'tp')
All inputs are finite; a program needn't handle non-finite values.
Results may differ from a plain program's by a relative error of at most 0.035.
Values may be sent and summed in bfloat16 or wider, within the bound.
A program may use at most 64 MiB of HBM per device.

v0:
```python
import jax
import jax.numpy as jnp
from jax import lax
from jax.sharding import PartitionSpec as P


def rotate(part, positions):
    half = part.shape[-1] // 2
    freqs = 1.0 / 10000.0 ** (jnp.arange(half, dtype=jnp.float32) * 2.0 / part.shape[-1])
    angles = positions.astype(jnp.float32)[:, None] * freqs
    cosine = jnp.cos(angles)
    sine = jnp.sin(angles)
    first = part[..., :half]
    second = part[..., half:]
    return jnp.concatenate(
        [first * cosine - second * sine, second * cosine + first * sine], axis=-1
    )


def body(
    tokens,
    latent_down_matrix,
    rope_weight,
    latent_norm_scale,
    key_up_matrix,
    value_up_matrix,
    query,
):
    seq_count, span, width = tokens.shape
    flat = tokens.reshape(seq_count * span, width)
    lat_width = latent_down_matrix.shape[1]
    rope_width = rope_weight.shape[1]
    latent = jnp.dot(
        flat,
        lax.all_gather(latent_down_matrix, "tp", axis=0, tiled=True),
        preferred_element_type=jnp.float32,
    )
    rope = jnp.dot(
        flat,
        lax.all_gather(rope_weight, "tp", axis=0, tiled=True),
        preferred_element_type=jnp.float32,
    )
    scaled = latent * lax.rsqrt(jnp.mean(latent * latent, axis=-1, keepdims=True) + 1e-06)
    latent_normalized = (scaled * latent_norm_scale).astype(jnp.bfloat16)
    offset = lax.axis_index("sp") * span
    positions = offset + jnp.arange(span, dtype=jnp.int32)
    rope_key = rotate(rope.reshape(seq_count, span, rope_width), positions).astype(jnp.bfloat16)
    packed = jnp.concatenate(
        [latent_normalized.reshape(seq_count, span, lat_width), rope_key], axis=-1
    )
    heads = key_up_matrix.shape[1]
    key_width = key_up_matrix.shape[2]
    val_width = value_up_matrix.shape[2]
    head_width = key_width + val_width
    up_weight = jnp.concatenate([key_up_matrix, value_up_matrix], axis=-1).reshape(
        lat_width, heads * head_width
    )
    collected = lax.all_gather(packed, "tp", axis=0, tiled=True)
    arrived = lax.all_to_all(collected, "sp", split_axis=0, concat_axis=1, tiled=True)
    lead = arrived.shape[:-1]
    product = jnp.dot(
        arrived[..., :lat_width].reshape(-1, lat_width),
        up_weight,
        preferred_element_type=jnp.float32,
    ).astype(jnp.bfloat16)
    built = jnp.concatenate(
        [product.reshape(lead + (heads * head_width,)), arrived[..., lat_width:]], axis=-1
    )
    kept, length = (built.shape[0], built.shape[1])
    per_head = built[..., : heads * head_width].reshape(kept, length, heads, head_width)
    plain_key_cache = per_head[..., :key_width]
    head_value_cache = per_head[..., key_width:]
    rotated_key_cache = built[..., heads * head_width :]
    query_plain = query[..., :key_width]
    rotated_query = rotate(
        query[..., key_width:].astype(jnp.float32), jnp.full((1,), length, jnp.int32)
    ).astype(jnp.bfloat16)
    factor = 1.0 / (key_width + rope_width) ** 0.5
    scores = jnp.einsum(
        "shd,slhd->shl", query_plain, plain_key_cache, preferred_element_type=jnp.float32
    )
    scores = scores + jnp.einsum(
        "ikg,ivg->ikv", rotated_query, rotated_key_cache, preferred_element_type=jnp.float32
    )
    scores = scores * factor
    weights = jnp.exp(scores - jnp.max(scores, axis=-1, keepdims=True))
    total = jnp.sum(weights, axis=-1, keepdims=True)
    mixed = jnp.einsum(
        "shl,slhd->shd",
        weights.astype(jnp.bfloat16),
        head_value_cache,
        preferred_element_type=jnp.float32,
    )
    first_read = (mixed / total).astype(jnp.bfloat16)
    return (plain_key_cache, head_value_cache, rotated_key_cache, first_read)


def solution(mesh):
    in_specs = (
        P("tp", "sp", None),
        P("tp", None),
        P("tp", None),
        P(),
        P(None, "tp", None),
        P(None, "tp", None),
        P("sp", "tp", None),
    )
    out_specs = (
        P("sp", None, "tp", None),
        P("sp", None, "tp", None),
        P("sp", None, None),
        P("sp", "tp", None),
    )
    return jax.shard_map(body, mesh=mesh, in_specs=in_specs, out_specs=out_specs, check_vma=False)
```

profile of v0, /device:TPU:0, one launch (start us, length us, event | category | flops | bytes accessed | tf_op | source)
XLA Modules:
  0.0 127.2 jit_solution(13641075231820190053)
XLA Ops:
  7.2 0.0 copy-start
  7.2 0.0 all-gather.3.cloned.1.call-start
  7.2 0.7 all-gather.3.cloned.1.call-update
  7.9 0.0 all-gather.5.cloned.1.call-start
  8.0 16.7 %all_gather.10 = bf16[4096,64]{0,1:T(8,128)(2,1)S(1)} all-gather(bf16[512,64]{0,1:T(8,128)(2,1)} %param.9), channel_id=1, replica_groups=mesh['sp'=4,'tp'=8] {'tp'}, dimensions={0}, use_global_device_ids=true | all-gather | bytes 589824 | tf_op jit(solution)/shard_map/all_gather | solution.py:40
  24.7 0.0 copy-done
  24.7 0.5 convolution_bitcast_fusion
  25.2 0.1 fusion.17
  25.4 0.1 copy.20
  25.5 0.1 copy.21
  25.6 0.0 copy-start.7
  25.6 33.7 %all-gather.3.cloned.1.call-done = bf16[4096,512]{1,0:T(8,128)(2,1)} async-done(((bf16[512,512]{1,0:T(8,128)(2,1)}), bf16[4096,512]{1,0:T(8,128)(2,1)}) %all-gather.3.cloned.1.call-update) | async-done | bytes 4194320 | tf_op jit(solution)/shard_map/all_gather | solution.py:35
  59.3 3.0 %multiply_reduce_fusion = (f32[128]{0:T(128)S(1)}, f32[128,512]{1,0:T(8,128)S(1)}) fusion(bf16[4096,512]{1,0:T(8,128)(2,1)} %all-gather.3.cloned.1.call-done, bf16[1,128,4096]{2,1,0:T(8,128)(2,1)S(1)} %copy-done), kind=kOutput, calls=%fused_computation.17 | convolution fusion | flops 537001856 | bytes 5505536 | tf_op jit(solution)/shard_map/dot_general | solution.py:33
  62.3 0.0 copy-start.4
  62.3 0.0 copy-start.5
  62.3 0.0 copy-done.7
  62.3 0.1 fusion.11
  62.4 0.1 pad_maximum_fusion.1
  62.5 0.8 copy.22
  63.3 0.0 all-gather.5.cloned.1.call-update
  63.3 22.2 %all-gather.5.cloned.1.call-done = bf16[8,128,576]{1,2,0:T(8,128)(2,1)} async-done(((bf16[1,128,576]{1,2,0:T(8,128)(2,1)}), bf16[8,128,576]{1,2,0:T(8,128)(2,1)}) %all-gather.5.cloned.1.call-update) | async-done | bytes 1179664 | tf_op jit(solution)/shard_map/all_gather | solution.py:58
  85.5 3.5 %all-to-all-start = ((bf16[8,128,576]{1,2,0:T(8,128)(2,1)}), bf16[8,128,576]{1,2,0:T(8,128)(2,1)S(1)}, u32[]{:S(2)}, u32[]{:S(2)}) async-start(bf16[8,128,576]{1,2,0:T(8,128)(2,1)} %all-gather.5.cloned.1.call-done), calls=%async_computation | async-start | bytes 2359296 | tf_op jit(solution)/shard_map/all_to_all | solution.py:59
  89.1 0.0 copy-done.4
  89.1 0.0 copy-done.5
  89.1 0.0 copy-start.6
  89.1 0.6 pad_maximum_fusion
  89.7 1.2 copy.31
  90.9 0.0 copy-done.6
  90.9 0.1 subtract_convert_fusion
  91.0 13.7 %all-to-all-done = bf16[8,128,576]{1,2,0:T(8,128)(2,1)S(1)} async-done(((bf16[8,128,576]{1,2,0:T(8,128)(2,1)}), bf16[8,128,576]{1,2,0:T(8,128)(2,1)S(1)}, u32[]{:S(2)}, u32[]{:S(2)}) %all-to-all-start) | async-done | bytes 1179680 | tf_op jit(solution)/shard_map/all_to_all | solution.py:59
  104.7 0.9 copy.44
  105.7 0.5 all_to_all.16
  106.2 0.0 copy-start.3
  106.2 0.1 slice.42
  106.3 0.0 copy-start.1
  106.3 1.3 %copy.24 = bf16[2,512,512]{2,1,0:T(8,128)(2,1)} copy(bf16[2,512,512]{1,2,0:T(8,128)(2,1)S(1)} %slice.42) | data formatting | bytes 2097152 | tf_op jit(solution)/shard_map/slice | solution.py:62
  107.6 0.0 copy-done.1
  107.6 3.8 %convolution_convert_fusion = bf16[1024,1024]{1,0:T(8,128)(2,1)} fusion(bf16[1024,512]{1,0:T(8,128)(2,1)} %bitcast.39, bf16[512,1024]{1,0:T(8,128)(2,1)S(1)} %bitcast.38), kind=kOutput, calls=%fused_computation.1 | convolution fusion | flops 1074790400 | bytes 4194304 | tf_op jit(solution)/shard_map/dot_general | solution.py:61
  111.4 3.3 %reshape_reshape.3 = bf16[2,512,4,256]{3,2,1,0:T(4,128)(2,1)S(1)} reshape(bf16[1024,1024]{1,0:T(8,128)(2,1)} %convolution_convert_fusion) | data formatting | bytes 4194304 | tf_op jit(solution)/shard_map/reshape;reshape | solution.py:70
  114.7 1.7 %fusion.26 = (bf16[2,512,4,128]{3,2,1,0:T(4,128)(2,1)}, bf16[2,512,4,128]{3,2,1,0:T(4,128)(2,1)S(1)}) fusion(bf16[2,512,4,256]{3,2,1,0:T(4,128)(2,1)S(1)} %reshape_reshape.3), kind=kLoop, calls=%fused_computation.47 | loop fusion | bytes 4194304 | tf_op jit(solution)/shard_map/slice | solution.py:72
  116.4 0.0 copy-start.2
  116.4 1.0 copy-done.2
  117.4 0.4 fusion.9
  117.8 0.0 copy-done.3
  117.8 0.3 fusion.2
  118.1 0.1 fusion.27
  118.2 1.5 %fusion.7 = f32[2,4,1,128]{3,2,1,0:T(1,128)S(1)} fusion(bf16[2,512,4,128]{3,2,1,0:T(4,128)(2,1)} %get-tuple-element.4, bf16[2,4,512,1]{2,1,0,3:T(4,128)(2,1)S(1)} %get-tuple-element.9), kind=kOutput, calls=%fused_computation.12 | convolution fusion | flops 1048576 | bytes 1060864 | tf_op jit(solution)/shard_map/shl,slhd->shd/dot_general | solution.py:88
  119.6 0.7 divide_convert_fusion
  (7 shorter events, 0.1 us)
Async XLA Ops:
  7.2 17.5 %copy-start = (bf16[1,128,4096]{2,1,0:T(8,128)(2,1)S(1)}, bf16[1,128,4096]{2,1,0:T(8,128)(2,1)}, u32[]{:S(2)}) copy-start(bf16[1,128,4096]{2,1,0:T(8,128)(2,1)} %param.7) | copy-start | bytes 3145732
  7.2 52.1 %all-gather.3.cloned.1.call-start = ((), (), s32[]{:S(2)}) async-start(), calls=%async_computation.1 | async-start | bytes 4718592 | tf_op jit(solution)/shard_map/all_gather | solution.py:35
  7.9 77.6 %all-gather.5.cloned.1.call-start = ((), (), s32[]{:S(2)}) async-start(), calls=%async_computation.2 | async-start | bytes 1327104 | tf_op jit(solution)/shard_map/all_gather | solution.py:58
  25.6 36.7 %copy-start.7 = (f32[512]{0:T(512)S(1)}, f32[512]{0:T(512)}, u32[]{:S(2)}) copy-start(f32[512]{0:T(512)} %param.10) | copy-start | bytes 6148
  62.3 26.8 %copy-start.4 = (bf16[512,4,128]{2,1,0:T(4,128)(2,1)S(1)}, bf16[512,4,128]{2,1,0:T(4,128)(2,1)}, u32[]{:S(2)}) copy-start(bf16[512,4,128]{2,1,0:T(4,128)(2,1)} %param.12) | copy-start | bytes 1572868
  62.3 26.8 %copy-start.5 = (bf16[512,4,128]{2,1,0:T(4,128)(2,1)S(1)}, bf16[512,4,128]{2,1,0:T(4,128)(2,1)}, u32[]{:S(2)}) copy-start(bf16[512,4,128]{2,1,0:T(4,128)(2,1)} %param.11) | copy-start | bytes 1572868
  85.5 19.2 %all-to-all-start = ((bf16[8,128,576]{1,2,0:T(8,128)(2,1)}), bf16[8,128,576]{1,2,0:T(8,128)(2,1)S(1)}, u32[]{:S(2)}, u32[]{:S(2)}) async-start(bf16[8,128,576]{1,2,0:T(8,128)(2,1)} %all-gather.5.cloned.1.call-done), calls=%async_computation | async-start | bytes 2359296 | tf_op jit(solution)/shard_map/all_to_all | solution.py:59
  89.1 1.8 %copy-start.6 = (bf16[2,4,192]{2,1,0:T(4,128)(2,1)S(1)}, bf16[2,4,192]{2,1,0:T(4,128)(2,1)}, u32[]{:S(2)}) copy-start(bf16[2,4,192]{2,1,0:T(4,128)(2,1)} %param.13) | copy-start | bytes 9220
  106.2 11.6 %copy-start.3 = (bf16[2,512,64]{1,2,0:T(8,128)(2,1)}, bf16[2,512,64]{1,2,0:T(8,128)(2,1)S(1)}, u32[]{:S(2)}) copy-start(bf16[2,512,64]{1,2,0:T(8,128)(2,1)S(1)} %slice.45) | copy-start | bytes 393220
  106.3 1.3 %copy-start.1 = (bf16[64,8,4,256]{3,1,2,0:T(8,128)(2,1)S(1)}, bf16[64,8,4,256]{3,1,2,0:T(8,128)(2,1)}, u32[]{:S(2)}) copy-start(bf16[64,8,4,256]{3,1,2,0:T(8,128)(2,1)} %copy.31) | copy-start | bytes 3145732
  116.4 1.0 copy-start.2
Sparse Core Ops, SparseCore 0:
  9.6 49.6 all-gather.2
  63.5 22.0 all-gather.4
where the time goes:
time: 128 us; the launch traced here: 127 us
  waiting for transfers between devices  70.3 us (55%)
  blocking collectives  16.7 us (13%)
  between operations  14.3 us (11%)
  local copies, waits for them, and re-layouts  11.1 us (9%)
  matrix products  9.43 us (7%)
  starting transfers between devices  3.6 us (3%)
  other arithmetic  1.78 us (1%)
    all_gather x1, waiting for transfers between devices, body(): lax.all_gather(latent_down_matrix, 'tp', axis=0, tiled=True)  33.7 us
    all_gather x1, waiting for transfers between devices, body(): collected = lax.all_gather(packed, 'tp', axis=0, tiled=True)  22.2 us
    all_gather x1, blocking collectives, body(): lax.all_gather(rope_weight, 'tp', axis=0, tiled=True)  16.7 us
    all_to_all x1, waiting for transfers between devices, body(): lax.all_to_all(collected, 'sp', split_axis=0, concat_axis=1, tiled=True)  13.7 us
    dot_general x1, matrix products, body(): jnp.dot(arrived[..., :lat_width].reshape(-1, lat_width), up_weight, prefe...  3.8 us
    all_to_all x1, starting transfers between devices, body(): lax.all_to_all(collected, 'sp', split_axis=0, concat_axis=1, tiled=True)  3.53 us
    another operation x1, local copies, waits for them, and re-layouts, body(): built[..., :heads * head_width].reshape(kept, length, heads, head_width)  3.33 us
    dot_general x1, matrix products, body(): jnp.dot(flat, lax.all_gather(latent_down_matrix, 'tp', axis=0, tiled=True...  2.98 us
  transfers between devices with their start and end apart: 3, of which 3 were waited for; matrix products, arithmetic and copies ran while one was open for 2% of the time, Pallas kernels for 0%

commit v1 on v0

v1 whole, which is shorter than its diff:
```python
import functools

import numpy as np
import jax
import jax.numpy as jnp
from jax import lax
from jax.sharding import PartitionSpec as P
from jax.experimental import pallas as pl
from jax.experimental.pallas import tpu as pltpu

CORES = 2
BF16 = jnp.bfloat16
F32 = jnp.float32


def turn_tables(positions, width):
    half = width // 2
    freqs = (1.0 / np.float32(10000.0) ** (np.arange(half, dtype=np.float32) * np.float32(2.0) / np.float32(width))).astype(np.float32)
    angles = positions.astype(np.float32)[:, None] * freqs
    cosine = np.cos(angles).astype(np.float32)
    sine = np.sin(angles).astype(np.float32)
    return np.concatenate([cosine, cosine], -1), np.concatenate([-sine, sine], -1)


def turn(part, cosine, sine):
    half = part.shape[-1] // 2
    swapped = jnp.concatenate([part[:, half:], part[:, :half]], axis=-1)
    return part * cosine + swapped * sine


def move_kernel(planes, spots, tok, wl, wr, scale, cos_ref, sin_ref, kup, vup, x_out, up_out,
                tokens, wlat, wrope, acc, other, spread, kbuf, vbuf,
                tok_s, tok_r, own_s, z_s, z_r, x_s, x_r, y_s, y_r, dx_s, dx_r, dy_s, dy_r,
                acc_s, acc_r, g_s, g_r, f_s, f_r, p_s, p_r, up_s):
    s = lax.axis_index("sp")
    t = lax.axis_index("tp")
    z = t // CORES
    c = t % CORES
    rows, lat = wl.shape
    rope = wr.shape[1]
    span = tok.shape[1]
    quarter = rows // 4
    eighth = quarter // 2
    q = s % 4
    base = s - q

    def flip(bit):
        if bit == 1:
            return s + 1 - 2 * (s % 2)
        return s + 2 - 4 * ((s // 2) % 2)

    sx = flip(1)
    sy = flip(2)

    def dev(si, zi, ci):
        return {"sp": si, "tp": zi * CORES + ci}

    def remote(src, dst, ss, rs, where):
        return pltpu.make_async_remote_copy(
            src_ref=src, dst_ref=dst, send_sem=ss, recv_sem=rs,
            device_id=where, device_id_type=pl.DeviceIdType.MESH)

    def own_tok(u):
        cols = pl.ds(pl.multiple_of((u * CORES + c) * rows, 128), rows)
        return pltpu.make_async_copy(tok.at[0, :, cols], tokens.at[0, u], own_s.at[u])

    def part_tok(u):
        cols = pl.ds(pl.multiple_of((u * CORES + 1 - c) * rows, 128), rows)
        return remote(tok.at[0, :, cols], tokens.at[1, u], tok_s.at[u], tok_r.at[u], dev(s, z, 1 - c))

    own_wl = pltpu.make_async_copy(wl, wlat.at[z], own_s.at[planes])
    own_wr = pltpu.make_async_copy(wr, wrope.at[z], own_s.at[planes + 1])
    get_k = pltpu.make_async_copy(kup, kbuf, up_s.at[0])
    get_v = pltpu.make_async_copy(vup, vbuf, up_s.at[1])
    own_wl.start()
    own_wr.start()

    barrier = pltpu.get_barrier_semaphore()

    def greet(where):
        pl.semaphore_signal(barrier, inc=1, device_id=where, device_id_type=pl.DeviceIdType.MESH)

    for i in range(1, planes):
        greet(dev(s, lax.rem(z + i, planes), c))
    for i in range(1, spots):
        greet(dev(lax.rem(s + i, spots), z, c))
    greet(dev(s, z, 1 - c))
    for u in range(planes):
        own_tok(u).start()
    own_wl.wait()
    own_wr.wait()
    pl.semaphore_wait(barrier, planes - 1 + spots - 1 + 1)

    def piece(u, start, count, sems, rsems, where):
        start = pl.multiple_of(start, 16)
        a = remote(wlat.at[u, pl.ds(start, count)], wlat.at[u, pl.ds(start, count)],
                   sems.at[0, u], rsems.at[0, u], where)
        b = remote(wrope.at[u, pl.ds(start, count)], wrope.at[u, pl.ds(start, count)],
                   sems.at[1, u], rsems.at[1, u], where)
        return a, b

    def each(pair, what):
        for p in pair:
            getattr(p, what)()

    qx = q + 1 - 2 * (q % 2)
    qy = q + 2 - 4 * (q // 2)
    qd = 3 - q

    def z_up(u):
        return piece(u, q * quarter, quarter, z_s, z_r, dev(s, z + 1, c))

    def z_down(u):
        a, b = piece(u, q * quarter, quarter, z_s, z_r, dev(s, z - 1, c))
        return a, b

    def z_up_own():
        start = pl.multiple_of(q * quarter, 16)
        return (remote(wlat.at[z, pl.ds(start, quarter)], wlat.at[z, pl.ds(start, quarter)], z_s.at[2, 0], z_r.at[0, z], dev(s, z + 1, c)),
                remote(wrope.at[z, pl.ds(start, quarter)], wrope.at[z, pl.ds(start, quarter)], z_s.at[2, 1], z_r.at[1, z], dev(s, z + 1, c)))

    def x_copy(u):
        return piece(u, q * quarter, quarter, x_s, x_r, dev(sx, z, c))

    def y_copy(u):
        return piece(u, q * quarter, quarter, y_s, y_r, dev(sy, z, c))

    def x_in(u):
        return piece(u, qx * quarter, quarter, x_s, x_r, dev(sx, z, c))

    def y_in(u):
        return piece(u, qy * quarter, quarter, y_s, y_r, dev(sy, z, c))

    def dy_copy(u):
        return piece(u, qx * quarter, eighth, dy_s, dy_r, dev(sy, z, c))

    def dx_copy(u):
        return piece(u, qy * quarter + eighth, eighth, dx_s, dx_r, dev(sx, z, c))

    def dy_in(u):
        return piece(u, qd * quarter, eighth, dy_s, dy_r, dev(sy, z, c))

    def dx_in(u):
        return piece(u, qd * quarter + eighth, eighth, dx_s, dx_r, dev(sx, z, c))

    @pl.when(z + 1 < planes)
    def _():
        each(z_up_own(), "start")

    @pl.when(z > 0)
    def _():
        each(z_down(z), "start")

    for u in range(planes):
        part_tok(u).start()
    get_k.start()
    get_v.start()

    def block_dot(u):
        x = tokens[:, u].reshape(CORES * span, rows)
        return (jnp.dot(x, wlat[u], preferred_element_type=F32),
                jnp.dot(x, wrope[u], preferred_element_type=F32))

    def load_tokens(u):
        own_tok(u).wait()
        part_tok(u).wait()

    for u in range(planes):
        load_tokens(u)
    a, b = block_dot(z)
    acc[:, :, :lat] = a.reshape(CORES, span, lat)
    acc[:, :, lat:] = b.reshape(CORES, span, rope)

    def reshape_up():
        get_k.wait()
        get_v.wait()
        heads = kbuf.shape[1]
        kw = kbuf.shape[2]
        vw = vbuf.shape[2]
        k = kbuf[...].astype(F32)
        v = vbuf[...].astype(F32)
        for h in range(heads):
            up_out[:, h * kw:(h + 1) * kw] = k[:, h, :].astype(BF16)
            up_out[:, heads * kw + h * vw:heads * kw + (h + 1) * vw] = v[:, h, :].astype(BF16)

    def step(d, carry):
        for sign in (-1, 1):
            u = z + sign * d

            @pl.when((u >= 0) & (u < planes))
            def _():
                each(piece(u, q * quarter, quarter, z_s, z_r, dev(s, z, 1 - c)), "wait_recv")
                if sign < 0:
                    @pl.when(z + 1 < planes)
                    def _():
                        each(z_up(u), "start")
                else:
                    @pl.when(z > 0)
                    def _():
                        each(z_down(u), "start")
                each(x_copy(u), "start")
                each(y_copy(u), "start")
        for sign in (-1, 1):
            u = z + sign * (d - 1)

            @pl.when((u >= 0) & (u < planes) & (d > 1))
            def _():
                each(x_in(u), "wait_recv")
                each(dy_copy(u), "start")
                each(y_in(u), "wait_recv")
                each(dx_copy(u), "start")
        for sign in (-1, 1):
            u = z + sign * (d - 2)

            @pl.when((u >= 0) & (u < planes) & (d > 2))
            def _():
                each(dy_in(u), "wait_recv")
                each(dx_in(u), "wait_recv")
                a, b = block_dot(u)
                acc[:, :, :lat] += a.reshape(CORES, span, lat)
                acc[:, :, lat:] += b.reshape(CORES, span, rope)
        return carry

    reshape_up()
    lax.fori_loop(1, planes + 2, step, 0)

    swap = remote(acc.at[1], other, acc_s, acc_r, dev(s, z, 1 - c))
    swap.start()
    swap.wait()
    latent = acc[0, :, :lat] + other[:, :lat]
    ropes = acc[0, :, lat:] + other[:, lat:]
    scaled = latent * lax.rsqrt(jnp.mean(latent * latent, axis=-1, keepdims=True) + 1e-06)
    spread[z, :, :lat] = (scaled * scale[...]).astype(BF16)
    spread[z, :, lat:] = turn(ropes, cos_ref[...], sin_ref[...]).astype(BF16)

    def g_copy(u, zi, slot):
        return remote(spread.at[u], spread.at[u], g_s.at[slot, u], g_r.at[u], dev(s, zi, c))

    def f_copy(u):
        return remote(spread.at[u], x_out.at[c, s], f_s.at[u], f_r.at[s], dev(u, z, c))

    def f_in(si):
        return remote(spread.at[0], x_out.at[c, si], f_s.at[0], f_r.at[si], dev(si, z, c))

    def p_copy(si):
        return remote(x_out.at[c, si], x_out.at[c, si], p_s.at[si], p_r.at[si], dev(s, z, 1 - c))

    def p_in(si):
        return remote(x_out.at[1 - c, si], x_out.at[1 - c, si], p_s.at[si], p_r.at[si], dev(s, z, 1 - c))

    own_copy = pltpu.make_async_copy(spread.at[s], x_out.at[c, s], own_s.at[0])

    def g_up(u):
        return g_copy(u, z + 1, 0)

    def g_down(u):
        return g_copy(u, z - 1, 1)

    def deliver(u):
        @pl.when(u != s)
        def _():
            f_copy(u).start()

        @pl.when(u == s)
        def _():
            own_copy.start()

    @pl.when(z + 1 < planes)
    def _():
        g_up(z).start()

    @pl.when(z > 0)
    def _():
        g_down(z).start()

    deliver(z)

    def g_step(d, carry):
        for sign in (-1, 1):
            u = z + sign * d

            @pl.when((u >= 0) & (u < planes))
            def _():
                g_copy(u, z, 0).wait_recv()
                if sign < 0:
                    @pl.when(z + 1 < planes)
                    def _():
                        g_up(u).start()
                else:
                    @pl.when(z > 0)
                    def _():
                        g_down(u).start()
                deliver(u)
        return carry

    lax.fori_loop(1, planes, g_step, 0)
    own_copy.wait()
    p_copy(s).start()

    def p_step(i, carry):
        si = lax.rem(s + i, spots)
        f_in(si).wait_recv()
        p_copy(si).start()
        return carry

    lax.fori_loop(1, spots, p_step, 0)

    def p_drain(si, carry):
        p_in(si).wait_recv()
        p_copy(si).wait_send()
        return carry

    lax.fori_loop(0, spots, p_drain, 0)

    def drain(u, carry):
        @pl.when(u != s)
        def _():
            f_copy(u).wait_send()

        @pl.when((u <= z) & (z + 1 < planes))
        def _():
            g_up(u).wait_send()

        @pl.when((u >= z) & (z > 0))
        def _():
            g_down(u).wait_send()

        @pl.when((u < z) & (z + 1 < planes))
        def _():
            each(z_up(u), "wait_send")

        @pl.when((u >= z) & (z > 0))
        def _():
            each(z_down(u), "wait_send")

        @pl.when(u != z)
        def _():
            each(x_copy(u), "wait_send")
            each(y_copy(u), "wait_send")
            each(dy_copy(u), "wait_send")
            each(dx_copy(u), "wait_send")
        return carry

    lax.fori_loop(0, planes, drain, 0)

    @pl.when(z + 1 < planes)
    def _():
        each(z_up_own(), "wait_send")


def read_kernel(x_ref, up_ref, q_ref, cos_ref, sin_ref, plain_ref, value_ref, rot_ref, read_ref, wide):
    length = x_ref.shape[1]
    heads = q_ref.shape[1]
    lat = up_ref.shape[0]
    rope = x_ref.shape[2] - lat
    kw = q_ref.shape[2] - rope
    vw = up_ref.shape[1] // heads - kw
    rotated = x_ref[0, :, lat:]
    rot_ref[0] = rotated
    normed = x_ref[0, :, :lat]
    keys = jnp.dot(normed, up_ref[:, :heads * kw], preferred_element_type=F32)
    values = jnp.dot(normed, up_ref[:, heads * kw:], preferred_element_type=F32)
    for h in range(heads):
        wide[pl.ds(h, length, stride=heads), :] = keys[:, h * kw:(h + 1) * kw]
    plain_ref[0] = wide[...].astype(BF16)
    for h in range(heads):
        wide[pl.ds(h, length, stride=heads), :] = values[:, h * vw:(h + 1) * vw]
    value_ref[0] = wide[...].astype(BF16)
    keys = keys.astype(BF16)
    values = values.astype(BF16)
    query = q_ref[0].astype(F32)
    turned = turn(query[:, kw:], cos_ref[...], sin_ref[...]).astype(BF16)
    tiled = jnp.concatenate([query[:, :kw]] * heads, axis=1)
    row = lax.broadcasted_iota(jnp.int32, tiled.shape, 0)
    col = lax.broadcasted_iota(jnp.int32, tiled.shape, 1)
    blocked = jnp.where(col // kw == row, tiled, 0.0).astype(BF16)
    contract = (((1,), (1,)), ((), ()))
    scores = lax.dot_general(blocked, keys, contract, preferred_element_type=F32)
    scores = scores + lax.dot_general(turned, rotated, contract, preferred_element_type=F32)
    scores = scores * (1.0 / (kw + rope) ** 0.5)
    weights = jnp.exp(scores - jnp.max(scores, axis=-1, keepdims=True))
    total = jnp.sum(weights, axis=-1, keepdims=True)
    mixed = jnp.dot(weights.astype(BF16), values, preferred_element_type=F32) / total
    for h in range(heads):
        read_ref[0, h:h + 1, :] = mixed[h:h + 1, h * vw:(h + 1) * vw].astype(BF16)


def body(planes, spots, tokens, latent_down, rope_weight, norm_scale, key_up, value_up, query):
    span = tokens.shape[1]
    rows, lat = latent_down.shape
    rope = rope_weight.shape[1]
    heads, kw = key_up.shape[1:]
    vw = value_up.shape[2]
    length = spots * span
    cosine, sine = turn_tables(np.arange(length + 1), rope)
    s = lax.axis_index("sp")
    cos_here = lax.dynamic_slice_in_dim(jnp.asarray(cosine), s * span, span, 0)
    sin_here = lax.dynamic_slice_in_dim(jnp.asarray(sine), s * span, span, 0)
    vmem = pl.BlockSpec(memory_space=pltpu.VMEM)
    hbm = pl.BlockSpec(memory_space=pl.ANY)
    dma = pltpu.SemaphoreType.DMA
    x_all, up = pl.pallas_call(
        functools.partial(move_kernel, planes, spots),
        out_shape=(jax.ShapeDtypeStruct((CORES, spots, span, lat + rope), BF16),
                   jax.ShapeDtypeStruct((lat, heads * (kw + vw)), BF16)),
        in_specs=[hbm, vmem, vmem, vmem, vmem, vmem, hbm, hbm],
        out_specs=(vmem, vmem),
        scratch_shapes=[
            pltpu.VMEM((CORES, planes, span, rows), BF16),
            pltpu.VMEM((planes, rows, lat), BF16),
            pltpu.VMEM((planes, rows, rope), BF16),
            pltpu.VMEM((CORES, span, lat + rope), F32),
            pltpu.VMEM((span, lat + rope), F32),
            pltpu.VMEM((planes, span, lat + rope), BF16),
            pltpu.VMEM(key_up.shape, BF16),
            pltpu.VMEM(value_up.shape, BF16),
            dma((planes,)), dma((planes,)), dma((planes + 2,)),
            dma((3, max(planes, 2))), dma((2, planes)),
            dma((2, planes)), dma((2, planes)), dma((2, planes)), dma((2, planes)),
            dma((2, planes)), dma((2, planes)), dma((2, planes)), dma((2, planes)),
            dma, dma,
            dma((2, planes)), dma((planes,)),
            dma((planes,)), dma((spots,)),
            dma((spots,)), dma((spots,)),
            dma((2,)),
        ],
        compiler_params=pltpu.CompilerParams(collective_id=0, has_side_effects=True),
    )(tokens, latent_down, rope_weight, norm_scale.reshape(1, lat), cos_here, sin_here, key_up, value_up)
    x_all = x_all.reshape(CORES, length, lat + rope)

    def whole(shape):
        return pl.BlockSpec(shape, lambda i: (0,) * len(shape))

    def per(shape):
        return pl.BlockSpec((1,) + shape, lambda i: (i,) + (0,) * len(shape))

    plain, value, rot, read = pl.pallas_call(
        read_kernel,
        grid=(CORES,),
        out_shape=(jax.ShapeDtypeStruct((CORES, length * heads, kw), BF16),
                   jax.ShapeDtypeStruct((CORES, length * heads, vw), BF16),
                   jax.ShapeDtypeStruct((CORES, length, rope), BF16),
                   jax.ShapeDtypeStruct((CORES, heads, vw), BF16)),
        in_specs=[per((length, lat + rope)), whole(up.shape), per(query.shape[1:]), whole((1, rope)), whole((1, rope))],
        out_specs=(per((length * heads, kw)), per((length * heads, vw)), per((length, rope)), per((heads, vw))),
        scratch_shapes=[pltpu.VMEM((length * heads, kw), F32)],
    )(x_all, up, query, jnp.asarray(cosine[length:]), jnp.asarray(sine[length:]))
    return (plain.reshape(CORES, length, heads, kw), value.reshape(CORES, length, heads, vw), rot, read)


def solution(mesh):
    planes = mesh.shape["tp"] // CORES
    spots = mesh.shape["sp"]
    assert planes == spots and spots % 4 == 0
    in_specs = (
        P("tp", "sp", None),
        P("tp", None),
        P("tp", None),
        P(),
        P(None, "tp", None),
        P(None, "tp", None),
        P("sp", "tp", None),
    )
    out_specs = (
        P("sp", None, "tp", None),
        P("sp", None, "tp", None),
        P("sp", None, None),
        P("sp", "tp", None),
    )
    return jax.shard_map(functools.partial(body, planes, spots), mesh=mesh, in_specs=in_specs,
                         out_specs=out_specs, check_vma=False)
```

time: 128 us -> 67.1 us (0.52)
  the two profiles are of different devices: /device:TPU:0 before, /device:TPU:7 now
where the time goes in v1:
time: 67.1 us; the launch traced here: 66.4 us
  Pallas kernels  60.9 us (91%)
  local copies, waits for them, and re-layouts  4.91 us (7%)
    pallas_call x1, Pallas kernels, body(): pl.pallas_call(functools.partial(move_kernel, planes, spots), out_shape=(...  56.1 us
    pallas_call x1, Pallas kernels, body(): pl.pallas_call(read_kernel, grid=(CORES,), out_shape=(jax.ShapeDtypeStruc...  4.74 us
    unnamed x2, local copies, waits for them, and re-layouts  3.32 us
    dynamic_slice x1, local copies, waits for them, and re-layouts, body(): sin_here = lax.dynamic_slice_in_dim(jnp.asarray(sine), s * span, span, 0)  1.59 us

profile of v1, /device:TPU:7, one launch (start us, length us, event | category | flops | bytes accessed | tf_op | source)
XLA Modules:
  0.0 66.4 jit_solution(7331281912119795023)
XLA Ops:
  0.6 1.6 %constant_dynamic-slice_fusion = (f32[128,64]{1,0:T(8,128)}, f32[128,64]{1,0:T(8,128)}) fusion(f32[513,64]{1,0:T(8,128)} %constant.20.clone, s32[]{:T(128)S(6)} %select_n.4, f32[513,64]{1,0:T(8,128)} %constant.19.clone), kind=kLoop, calls=%fused_computation | loop fusion | bytes 131076 | tf_op jit(solution)/shard_map/dynamic_slice | solution.py:398
  2.2 1.6 %copy.15.wr = bf16[512,64]{1,0:T(8,128)(2,1)} copy(bf16[512,64]{0,1:T(8,128)(2,1)} %param.13) | data formatting | bytes 131072 | tf_op args[2]
  3.8 56.1 %shard_map.138 = (bf16[2,4,128,576]{3,2,1,0:T(8,128)(2,1)}, bf16[512,1024]{1,0:T(8,128)(2,1)}) custom-call(bf16[1,128,4096]{2,1,0:T(8,128)(2,1)} %tok.1, bf16[512,512]{1,0:T(8,128)(2,1)} %wl.1, bf16[512,64]{1,0:T(8,128)(2,1)} %copy.15.wr, f32[1,512]{1,0:T(1,128)} %bitcast.5, f32[128,64]{1,0:T(8,128)} %get-tuple-element.21.cos_ref, ...), custom_call_target="tpu_custom_call" | custom-call | tf_op jit(solution)/shard_map/pallas_call | solution.py:402
  60.0 4.7 %shard_map.139 = (bf16[2,2048,128]{2,1,0:T(8,128)(2,1)}, bf16[2,2048,128]{2,1,0:T(8,128)(2,1)}, bf16[2,512,64]{2,1,0:T(8,128)(2,1)}, bf16[2,4,128]{2,1,0:T(4,128)(2,1)}) custom-call(bf16[2,512,576]{2,1,0:T(8,128)(2,1)} %bitcast.4, bf16[512,1024]{1,0:T(8,128)(2,1)} %get-tuple-element.11.up_ref, bf16[2,4,192]{2,1,0:T(4,128)(2,1)} %q_ref.1, ...), custom_call_target="tpu_custom_call" | custom-call | tf_op jit(solution)/shard_map/pallas_call | solution.py:437
  64.7 1.7 %copy.16 = bf16[2,512,64]{1,2,0:T(8,128)(2,1)} copy(bf16[2,512,64]{2,1,0:T(8,128)(2,1)} %get-tuple-element.18) | data formatting | bytes 262144

commit v2 on v1

v2 whole, which is shorter than its diff:
```python
import functools

import numpy as np
import jax
import jax.numpy as jnp
from jax import lax
from jax.sharding import PartitionSpec as P
from jax.experimental import pallas as pl
from jax.experimental.pallas import tpu as pltpu

CORES = 2
BF16 = jnp.bfloat16
F32 = jnp.float32


def turn_tables(positions, width):
    half = width // 2
    freqs = (1.0 / np.float32(10000.0) ** (np.arange(half, dtype=np.float32) * np.float32(2.0) / np.float32(width))).astype(np.float32)
    angles = positions.astype(np.float32)[:, None] * freqs
    cosine = np.cos(angles).astype(np.float32)
    sine = np.sin(angles).astype(np.float32)
    return np.concatenate([cosine, cosine], -1), np.concatenate([-sine, sine], -1)


def turn(part, cosine, sine):
    half = part.shape[-1] // 2
    swapped = jnp.concatenate([part[:, half:], part[:, :half]], axis=-1)
    return part * cosine + swapped * sine


def move_kernel(planes, spots, tok, wl, wr, scale, cos_hbm, sin_hbm, kup, vup, x_out, rot_out, up_out,
                tokens, wlat, wrope, acc, acct, other, othert, spread, spreadt, kbuf, vbuf, cos_ref, sin_ref,
                tok_s, tok_r, own_s, z_s, z_r, zo_s, x_s, x_r, y_s, y_r, dx_s, dx_r, dy_s, dy_r,
                acc_s, acc_r, g_s, g_r, f_s, f_r, p_s, p_r, up_s):
    s = lax.axis_index("sp")
    t = lax.axis_index("tp")
    z = t // CORES
    c = t % CORES
    rows, lat = wl.shape
    rope = wr.shape[0]
    span = tok.shape[1]
    quarter = rows // 4
    eighth = quarter // 2
    rpart = rope // 4
    half = span // 2
    q = s % 4
    sx = s + 1 - 2 * (s % 2)
    sy = s + 2 - 4 * ((s // 2) % 2)
    qx = q + 1 - 2 * (q % 2)
    qy = q + 2 - 4 * (q // 2)
    qd = 3 - q

    def dev(si, zi, ci):
        return {"sp": si, "tp": zi * CORES + ci}

    here = dev(s, z, 1 - c)

    def remote(src, dst, ss, rs, where):
        return pltpu.make_async_remote_copy(
            src_ref=src, dst_ref=dst, send_sem=ss, recv_sem=rs,
            device_id=where, device_id_type=pl.DeviceIdType.MESH)

    def own_tok(u):
        cols = pl.ds(pl.multiple_of((u * CORES + c) * rows, 128), rows)
        return pltpu.make_async_copy(tok.at[0, :, cols], tokens.at[0, u], own_s.at[u])

    def part_tok(u):
        cols = pl.ds(pl.multiple_of((u * CORES + 1 - c) * rows, 128), rows)
        return remote(tok.at[0, :, cols], tokens.at[1, u], tok_s.at[u], tok_r.at[u], here)

    own_wl = pltpu.make_async_copy(wl, wlat.at[z], own_s.at[planes])
    own_wr = pltpu.make_async_copy(wr, wrope.at[z], own_s.at[planes + 1])
    place = pl.ds(pl.multiple_of(s * span, 128), span)
    get_k = pltpu.make_async_copy(kup, kbuf, up_s.at[0])
    get_v = pltpu.make_async_copy(vup, vbuf, up_s.at[1])
    get_c = pltpu.make_async_copy(cos_hbm.at[:, place], cos_ref, up_s.at[2])
    get_n = pltpu.make_async_copy(sin_hbm.at[:, place], sin_ref, up_s.at[3])
    own_wl.start()
    own_wr.start()

    barrier = pltpu.get_barrier_semaphore()

    def greet(where):
        pl.semaphore_signal(barrier, inc=1, device_id=where, device_id_type=pl.DeviceIdType.MESH)

    for i in range(1, planes):
        greet(dev(s, lax.rem(z + i, planes), c))
    for i in range(1, spots):
        greet(dev(lax.rem(s + i, spots), z, c))
    greet(here)
    for u in range(planes):
        own_tok(u).start()
    own_wl.wait()
    own_wr.wait()
    pl.semaphore_wait(barrier, planes - 1 + spots - 1 + 1)

    def piece(u, part, k, ss, rs, where):
        rng = pl.ds(pl.multiple_of(part * quarter + k * eighth, 16), eighth)
        out = [remote(wlat.at[u, rng], wlat.at[u, rng], ss.at[k, u], rs.at[k, u], where)]
        if k == 0:
            rng = pl.ds(pl.multiple_of(part * rpart, 16), rpart)
            out.append(remote(wrope.at[u, rng], wrope.at[u, rng], ss.at[2, u], rs.at[2, u], where))
        return out

    def each(copies, what):
        for p in copies:
            getattr(p, what)()

    def z_own(k):
        rng = pl.ds(pl.multiple_of(q * quarter + k * eighth, 16), eighth)
        where = dev(s, z + 1, c)
        out = [remote(wlat.at[z, rng], wlat.at[z, rng], zo_s.at[k], z_r.at[k, z], where)]
        if k == 0:
            rng = pl.ds(pl.multiple_of(q * rpart, 16), rpart)
            out.append(remote(wrope.at[z, rng], wrope.at[z, rng], zo_s.at[2], z_r.at[2, z], where))
        return out

    def z_up(u, k):
        return piece(u, q, k, z_s, z_r, dev(s, z + 1, c))

    def z_down(u, k):
        return piece(u, q, k, z_s, z_r, dev(s, z - 1, c))

    def x_copy(u, k):
        return piece(u, q, k, x_s, x_r, dev(sx, z, c))

    def y_copy(u, k):
        return piece(u, q, k, y_s, y_r, dev(sy, z, c))

    def x_in(u, k):
        return piece(u, qx, k, x_s, x_r, here)

    def y_in(u, k):
        return piece(u, qy, k, y_s, y_r, here)

    def dy_copy(u):
        return piece(u, qx, 0, dy_s, dy_r, dev(sy, z, c))

    def dx_copy(u):
        return piece(u, qy, 1, dx_s, dx_r, dev(sx, z, c))

    def dy_in(u):
        return piece(u, qd, 0, dy_s, dy_r, here)

    def dx_in(u):
        return piece(u, qd, 1, dx_s, dx_r, here)

    has_up = z + 1 < planes
    has_down = z > 0
    for k in range(2):
        @pl.when(has_up)
        def _():
            each(z_own(k), "start")

        @pl.when(has_down)
        def _():
            each(z_down(z, k), "start")

    for u in range(planes):
        part_tok(u).start()
    get_k.start()
    get_v.start()
    get_c.start()
    get_n.start()
    contract = (((1,), (1,)), ((), ()))

    def block_dot(u):
        x = tokens[:, u].reshape(CORES * span, rows)
        return (jnp.dot(x, wlat[u], preferred_element_type=F32),
                lax.dot_general(wrope[u], x, contract, preferred_element_type=F32))

    for u in range(planes):
        own_tok(u).wait()
        part_tok(u).wait()
    a, b = block_dot(z)
    acc[...] = a
    acct[...] = b
    get_k.wait()
    get_v.wait()
    get_c.wait()
    get_n.wait()

    def reshape_up():
        heads, kw = kbuf.shape[1:]
        vw = vbuf.shape[2]
        k = kbuf[...].astype(F32)
        v = vbuf[...].astype(F32)
        for h in range(heads):
            up_out[:, h * kw:(h + 1) * kw] = k[:, h, :].astype(BF16)
            up_out[:, heads * kw + h * vw:heads * kw + (h + 1) * vw] = v[:, h, :].astype(BF16)

    def step(d, carry):
        for k in range(2):
            for sign in (-1, 1):
                u = z + sign * d

                @pl.when((u >= 0) & (u < planes))
                def _():
                    each(piece(u, q, k, z_s, z_r, here), "wait_recv")
                    if sign < 0:
                        @pl.when(has_up)
                        def _():
                            each(z_up(u, k), "start")
                    else:
                        @pl.when(has_down)
                        def _():
                            each(z_down(u, k), "start")
                    each(x_copy(u, k), "start")
                    each(y_copy(u, k), "start")

        @pl.when(d == 1)
        def _():
            reshape_up()

        for sign in (-1, 1):
            u = z + sign * (d - 1)

            @pl.when((u >= 0) & (u < planes) & (d > 1))
            def _():
                each(x_in(u, 0), "wait_recv")
                each(dy_copy(u), "start")
                each(y_in(u, 1), "wait_recv")
                each(dx_copy(u), "start")
        for sign in (-1, 1):
            u = z + sign * (d - 2)

            @pl.when((u >= 0) & (u < planes) & (d > 2))
            def _():
                each(x_in(u, 1), "wait_recv")
                each(y_in(u, 0), "wait_recv")
                each(dy_in(u), "wait_recv")
                each(dx_in(u), "wait_recv")
                a, b = block_dot(u)
                acc[...] += a
                acct[...] += b
        return carry

    lax.fori_loop(1, planes + 2, step, 0)

    swaps = [remote(acc.at[pl.ds(span, span)], other, acc_s.at[0], acc_r.at[0], here),
             remote(acct.at[:, pl.ds(span, span)], othert, acc_s.at[1], acc_r.at[1], here)]
    each(swaps, "start")
    each(swaps, "wait")
    latent = acc[:span] + other[...]
    ropes = acct[:, :span] + othert[...]
    scaled = latent * lax.rsqrt(jnp.mean(latent * latent, axis=-1, keepdims=True) + 1e-06)
    spread[z] = (scaled * scale[...]).astype(BF16)
    swapped = jnp.concatenate([ropes[rope // 2:], ropes[:rope // 2]], axis=0)
    spreadt[z] = (ropes * cos_ref[...] + swapped * sin_ref[...]).astype(BF16)

    def g_copy(u, k, zi, slot):
        rng = pl.ds(k * half, half)
        out = [remote(spread.at[u, rng], spread.at[u, rng], g_s.at[slot, k, u], g_r.at[k, u], dev(s, zi, c))]
        if k == 0:
            out.append(remote(spreadt.at[u], spreadt.at[u], g_s.at[slot, 2, u], g_r.at[2, u], dev(s, zi, c)))
        return out

    def lanes(si):
        return pl.ds(pl.multiple_of(si * span, 128), span)

    def f_copy(u, k, where, si):
        rng = pl.ds(k * half, half)
        out = [remote(spread.at[u, rng], x_out.at[c, si, rng], f_s.at[k, u], f_r.at[k, si], where)]
        if k == 0:
            out.append(remote(spreadt.at[u], rot_out.at[c, :, lanes(si)], f_s.at[2, u], f_r.at[2, si], where))
        return out

    def p_copy(ci, si, k):
        rng = pl.ds(k * half, half)
        out = [remote(x_out.at[ci, si, rng], x_out.at[ci, si, rng], p_s.at[k, si], p_r.at[k, si], here)]
        if k == 0:
            part = rot_out.at[ci, :, lanes(si)]
            out.append(remote(part, part, p_s.at[2, si], p_r.at[2, si], here))
        return out

    own_copies = [pltpu.make_async_copy(spread.at[s], x_out.at[c, s], own_s.at[0]),
                  pltpu.make_async_copy(spreadt.at[s], rot_out.at[c, :, lanes(s)], own_s.at[1])]

    def deliver(u, k):
        @pl.when(u != s)
        def _():
            each(f_copy(u, k, dev(u, z, c), s), "start")

        if k == 1:
            @pl.when(u == s)
            def _():
                each(own_copies, "start")

    for k in range(2):
        @pl.when(has_up)
        def _():
            each(g_copy(z, k, z + 1, 0), "start")

        @pl.when(has_down)
        def _():
            each(g_copy(z, k, z - 1, 1), "start")

        deliver(z, k)

    def g_step(d, carry):
        for k in range(2):
            for sign in (-1, 1):
                u = z + sign * d

                @pl.when((u >= 0) & (u < planes))
                def _():
                    each(g_copy(u, k, z, 0), "wait_recv")
                    if sign < 0:
                        @pl.when(has_up)
                        def _():
                            each(g_copy(u, k, z + 1, 0), "start")
                    else:
                        @pl.when(has_down)
                        def _():
                            each(g_copy(u, k, z - 1, 1), "start")
                    deliver(u, k)
        return carry

    lax.fori_loop(1, planes, g_step, 0)
    each(own_copies, "wait")
    for k in range(2):
        each(p_copy(c, s, k), "start")

    def p_step(i, carry):
        si = lax.rem(s + i, spots)
        for k in range(2):
            each(f_copy(0, k, here, si), "wait_recv")
            each(p_copy(c, si, k), "start")
        return carry

    lax.fori_loop(1, spots, p_step, 0)

    def p_drain(si, carry):
        for k in range(2):
            each(p_copy(1 - c, si, k), "wait_recv")
            each(p_copy(c, si, k), "wait_send")
        return carry

    lax.fori_loop(0, spots, p_drain, 0)

    def drain(u, carry):
        for k in range(2):
            @pl.when(u != s)
            def _():
                each(f_copy(u, k, here, s), "wait_send")

            @pl.when((u <= z) & has_up)
            def _():
                each(g_copy(u, k, z, 0), "wait_send")

            @pl.when((u >= z) & has_down)
            def _():
                each(g_copy(u, k, z, 1), "wait_send")
                each(z_down(u, k), "wait_send")

            @pl.when((u < z) & has_up)
            def _():
                each(z_up(u, k), "wait_send")

            @pl.when(u != z)
            def _():
                each(x_copy(u, k), "wait_send")
                each(y_copy(u, k), "wait_send")

        @pl.when(u != z)
        def _():
            each(dy_copy(u), "wait_send")
            each(dx_copy(u), "wait_send")
        return carry

    lax.fori_loop(0, planes, drain, 0)

    @pl.when(has_up)
    def _():
        for k in range(2):
            each(z_own(k), "wait_send")


def read_kernel(x_ref, r_ref, up_ref, q_ref, cos_ref, sin_ref, plain_ref, value_ref, rot_ref, read_ref, wide):
    length = x_ref.shape[1]
    heads = q_ref.shape[1]
    lat = up_ref.shape[0]
    rope = r_ref.shape[1]
    kw = q_ref.shape[2] - rope
    vw = up_ref.shape[1] // heads - kw
    rotated = r_ref[0]
    rot_ref[0] = rotated
    normed = x_ref[0]
    keys = jnp.dot(normed, up_ref[:, :heads * kw], preferred_element_type=F32)
    values = jnp.dot(normed, up_ref[:, heads * kw:], preferred_element_type=F32)
    for h in range(heads):
        wide[pl.ds(h, length, stride=heads), :] = keys[:, h * kw:(h + 1) * kw]
    plain_ref[0] = wide[...].astype(BF16)
    for h in range(heads):
        wide[pl.ds(h, length, stride=heads), :] = values[:, h * vw:(h + 1) * vw]
    value_ref[0] = wide[...].astype(BF16)
    keys = keys.astype(BF16)
    values = values.astype(BF16)
    query = q_ref[0].astype(F32)
    turned = turn(query[:, kw:], cos_ref[...], sin_ref[...]).astype(BF16)
    tiled = jnp.concatenate([query[:, :kw]] * heads, axis=1)
    row = lax.broadcasted_iota(jnp.int32, tiled.shape, 0)
    col = lax.broadcasted_iota(jnp.int32, tiled.shape, 1)
    blocked = jnp.where(col // kw == row, tiled, 0.0).astype(BF16)
    contract = (((1,), (1,)), ((), ()))
    scores = lax.dot_general(blocked, keys, contract, preferred_element_type=F32)
    scores = scores + jnp.dot(turned, rotated, preferred_element_type=F32)
    scores = scores * (1.0 / (kw + rope) ** 0.5)
    weights = jnp.exp(scores - jnp.max(scores, axis=-1, keepdims=True))
    total = jnp.sum(weights, axis=-1, keepdims=True)
    mixed = jnp.dot(weights.astype(BF16), values, preferred_element_type=F32) / total
    for h in range(heads):
        read_ref[0, h:h + 1, :] = mixed[h:h + 1, h * vw:(h + 1) * vw].astype(BF16)


def body(planes, spots, tokens, latent_down, rope_weight, norm_scale, key_up, value_up, query):
    span = tokens.shape[1]
    rows, lat = latent_down.shape
    rope = rope_weight.shape[1]
    heads, kw = key_up.shape[1:]
    vw = value_up.shape[2]
    length = spots * span
    cosine, sine = turn_tables(np.arange(length + 1), rope)
    vmem = pl.BlockSpec(memory_space=pltpu.VMEM)
    hbm = pl.BlockSpec(memory_space=pl.ANY)
    dma = pltpu.SemaphoreType.DMA
    x_all, rot_all, up = pl.pallas_call(
        functools.partial(move_kernel, planes, spots),
        out_shape=(jax.ShapeDtypeStruct((CORES, spots, span, lat), BF16),
                   jax.ShapeDtypeStruct((CORES, rope, length), BF16),
                   jax.ShapeDtypeStruct((lat, heads * (kw + vw)), BF16)),
        in_specs=[hbm, hbm, hbm, vmem, hbm, hbm, hbm, hbm],
        out_specs=(vmem, vmem, vmem),
        scratch_shapes=[
            pltpu.VMEM((CORES, planes, span, rows), BF16),
            pltpu.VMEM((planes, rows, lat), BF16),
            pltpu.VMEM((planes, rope, rows), BF16),
            pltpu.VMEM((CORES * span, lat), F32),
            pltpu.VMEM((rope, CORES * span), F32),
            pltpu.VMEM((span, lat), F32),
            pltpu.VMEM((rope, span), F32),
            pltpu.VMEM((planes, span, lat), BF16),
            pltpu.VMEM((planes, rope, span), BF16),
            pltpu.VMEM(key_up.shape, BF16),
            pltpu.VMEM(value_up.shape, BF16),
            pltpu.VMEM((rope, span), F32),
            pltpu.VMEM((rope, span), F32),
            dma((planes,)), dma((planes,)), dma((planes + 2,)),
            dma((3, planes)), dma((3, planes)), dma((3,)),
            dma((3, planes)), dma((3, planes)), dma((3, planes)), dma((3, planes)),
            dma((3, planes)), dma((3, planes)), dma((3, planes)), dma((3, planes)),
            dma((2,)), dma((2,)),
            dma((2, 3, planes)), dma((3, planes)),
            dma((3, planes)), dma((3, spots)),
            dma((3, spots)), dma((3, spots)),
            dma((4,)),
        ],
        compiler_params=pltpu.CompilerParams(collective_id=0, has_side_effects=True),
    )(tokens, latent_down, rope_weight.T, norm_scale.reshape(1, lat),
      jnp.asarray(np.ascontiguousarray(cosine[:length].T)), jnp.asarray(np.ascontiguousarray(sine[:length].T)),
      key_up, value_up)
    x_all = x_all.reshape(CORES, length, lat)

    def whole(shape):
        return pl.BlockSpec(shape, lambda i: (0,) * len(shape))

    def per(shape):
        return pl.BlockSpec((1,) + shape, lambda i: (i,) + (0,) * len(shape))

    plain, value, rot, read = pl.pallas_call(
        read_kernel,
        grid=(CORES,),
        out_shape=(jax.ShapeDtypeStruct((CORES, length * heads, kw), BF16),
                   jax.ShapeDtypeStruct((CORES, length * heads, vw), BF16),
                   jax.ShapeDtypeStruct((CORES, rope, length), BF16),
                   jax.ShapeDtypeStruct((CORES, heads, vw), BF16)),
        in_specs=[per((length, lat)), per((rope, length)), whole(up.shape), per(query.shape[1:]), whole((1, rope)), whole((1, rope))],
        out_specs=(per((length * heads, kw)), per((length * heads, vw)), per((rope, length)), per((heads, vw))),
        scratch_shapes=[pltpu.VMEM((length * heads, kw), F32)],
    )(x_all, rot_all, up, query, jnp.asarray(cosine[length:]), jnp.asarray(sine[length:]))
    return (plain.reshape(CORES, length, heads, kw), value.reshape(CORES, length, heads, vw), jnp.swapaxes(rot, 1, 2), read)


def solution(mesh):
    planes = mesh.shape["tp"] // CORES
    spots = mesh.shape["sp"]
    assert planes == spots and spots % 4 == 0
    in_specs = (
        P("tp", "sp", None),
        P("tp", None),
        P("tp", None),
        P(),
        P(None, "tp", None),
        P(None, "tp", None),
        P("sp", "tp", None),
    )
    out_specs = (
        P("sp", None, "tp", None),
        P("sp", None, "tp", None),
        P("sp", None, None),
        P("sp", "tp", None),
    )
    return jax.shard_map(functools.partial(body, planes, spots), mesh=mesh, in_specs=in_specs,
                         out_specs=out_specs, check_vma=False)
```

time: 67.1 us -> 55.5 us (0.83)
  Pallas kernels: 60.9 us -> 54.6 us
  local copies, waits for them, and re-layouts: 4.91 us -> 0 us
    pallas_call x1, Pallas kernels: 56.1 us -> 50 us  [body(): pl.pallas_call(functools.partial(move_kernel, planes, spots), out_shape=(...]
    unnamed x2 -> x0, local copies, waits for them, and re-layouts: 3.32 us -> none
    dynamic_slice x1 -> x0, local copies, waits for them, and re-layouts: 1.59 us -> none  [body(): sin_here = lax.dynamic_slice_in_dim(jnp.asarray(sine), s * span, span, 0)]
where the time goes in v2:
time: 55.5 us; the launch traced here: 55.3 us
  Pallas kernels  54.6 us (98%)
  between operations  0.64 us (1%)
    pallas_call x1, Pallas kernels, body(): pl.pallas_call(functools.partial(move_kernel, planes, spots), out_shape=(...  50 us
    pallas_call x1, Pallas kernels, body(): pl.pallas_call(read_kernel, grid=(CORES,), out_shape=(jax.ShapeDtypeStruc...  4.65 us

profile of v2, /device:TPU:7, one launch (start us, length us, event | category | flops | bytes accessed | tf_op | source)
XLA Modules:
  0.0 55.3 jit_solution(970252595778168797)
XLA Ops:
  0.6 50.0 %shard_map.138 = (bf16[2,4,128,512]{3,2,1,0:T(8,128)(2,1)}, bf16[2,64,512]{2,1,0:T(8,128)(2,1)}, bf16[512,1024]{1,0:T(8,128)(2,1)}) custom-call(bf16[1,128,4096]{2,1,0:T(8,128)(2,1)} %tok.1, bf16[512,512]{1,0:T(8,128)(2,1)} %wl.1, bf16[64,512]{1,0:T(8,128)(2,1)} %bitcast.7, f32[1,512]{1,0:T(1,128)} %bitcast.8, f32[64,512]{1,0:T(8,128)} %constant.8.clone.cos_hbm, ...), custom_call_target="tpu_custom_call" | custom-call | tf_op jit(solution)/shard_map/pallas_call | solution.py:427
  50.6 4.7 %shard_map.139 = (bf16[2,2048,128]{2,1,0:T(8,128)(2,1)}, bf16[2,2048,128]{2,1,0:T(8,128)(2,1)}, bf16[2,64,512]{2,1,0:T(8,128)(2,1)}, bf16[2,4,128]{2,1,0:T(4,128)(2,1)}) custom-call(bf16[2,512,512]{2,1,0:T(8,128)(2,1)} %bitcast.6, bf16[2,64,512]{2,1,0:T(8,128)(2,1)} %get-tuple-element.12.r_ref, bf16[512,1024]{1,0:T(8,128)(2,1)} %get-tuple-element.13.up_ref, ...), custom_call_target="tpu_custom_call" | custom-call | tf_op jit(solution)/shard_map/pallas_call | solution.py:470

commit v3 on v2

--- a/solution.py
+++ b/solution.py
@@ -9,6 +9,7 @@
 from jax.experimental.pallas import tpu as pltpu
 
 CORES = 2
+PARTS = 4
 BF16 = jnp.bfloat16
 F32 = jnp.float32
 
@@ -42,7 +43,7 @@
     quarter = rows // 4
     eighth = quarter // 2
     rpart = rope // 4
-    half = span // 2
+    half = span // PARTS
     q = s % 4
     sx = s + 1 - 2 * (s % 2)
     sy = s + 2 - 4 * ((s // 2) % 2)
@@ -106,20 +107,33 @@
         for p in copies:
             getattr(p, what)()
 
-    def z_own(k):
-        rng = pl.ds(pl.multiple_of(q * quarter + k * eighth, 16), eighth)
-        where = dev(s, z + 1, c)
-        out = [remote(wlat.at[z, rng], wlat.at[z, rng], zo_s.at[k], z_r.at[k, z], where)]
+    def z_rows(k):
+        start = q * quarter + k * eighth if k < 2 else qd * quarter + eighth
+        return pl.ds(pl.multiple_of(start, 16), eighth)
+
+    def z_piece(u, k, sems, where):
+        rng = z_rows(k)
+        i = k if k < 2 else 3
+        out = [remote(wlat.at[u, rng], wlat.at[u, rng], sems(i), z_r.at[i, u], where)]
         if k == 0:
             rng = pl.ds(pl.multiple_of(q * rpart, 16), rpart)
-            out.append(remote(wrope.at[z, rng], wrope.at[z, rng], zo_s.at[2], z_r.at[2, z], where))
+            out.append(remote(wrope.at[u, rng], wrope.at[u, rng], sems(2), z_r.at[2, u], where))
         return out
 
+    def z_own(k):
+        return z_piece(z, k, lambda i: zo_s.at[i], dev(s, z + 1, c))
+
     def z_up(u, k):
-        return piece(u, q, k, z_s, z_r, dev(s, z + 1, c))
+        return z_piece(u, k, lambda i: z_s.at[i, u], dev(s, z + 1, c))
 
     def z_down(u, k):
-        return piece(u, q, k, z_s, z_r, dev(s, z - 1, c))
+        return z_piece(u, k, lambda i: z_s.at[i, u], dev(s, z - 1, c))
+
+    def z_in(u, k):
+        return z_piece(u, k, lambda i: z_s.at[i, u], here)
+
+    def by_y(u):
+        return (u + c) % 2 == 0
 
     def x_copy(u, k):
         return piece(u, q, k, x_s, x_r, dev(sx, z, c))
@@ -137,13 +151,13 @@
         return piece(u, qx, 0, dy_s, dy_r, dev(sy, z, c))
 
     def dx_copy(u):
-        return piece(u, qy, 1, dx_s, dx_r, dev(sx, z, c))
+        return piece(u, qy, 0, dx_s, dx_r, dev(sx, z, c))
 
     def dy_in(u):
         return piece(u, qd, 0, dy_s, dy_r, here)
 
     def dx_in(u):
-        return piece(u, qd, 1, dx_s, dx_r, here)
+        return piece(u, qd, 0, dx_s, dx_r, here)
 
     has_up = z + 1 < planes
     has_down = z > 0
@@ -189,22 +203,37 @@
             up_out[:, h * kw:(h + 1) * kw] = k[:, h, :].astype(BF16)
             up_out[:, heads * kw + h * vw:heads * kw + (h + 1) * vw] = v[:, h, :].astype(BF16)
 
+    def relay(u, k, sign):
+        each(z_in(u, k), "wait_recv")
+        if sign < 0:
+            @pl.when(has_up)
+            def _():
+                each(z_up(u, k), "start")
+        else:
+            @pl.when(has_down)
+            def _():
+                each(z_down(u, k), "start")
+
+    def send_own(k):
+        @pl.when(has_up)
+        def _():
+            each(z_own(k), "start")
+
+        @pl.when(has_down)
+        def _():
+            each(z_down(z, k), "start")
+
+    def valid(u):
+        return (u >= 0) & (u < planes)
+
     def step(d, carry):
         for k in range(2):
             for sign in (-1, 1):
                 u = z + sign * d
 
-                @pl.when((u >= 0) & (u < planes))
+                @pl.when(valid(u))
                 def _():
-                    each(piece(u, q, k, z_s, z_r, here), "wait_recv")
-                    if sign < 0:
-                        @pl.when(has_up)
-                        def _():
-                            each(z_up(u, k), "start")
-                    else:
-                        @pl.when(has_down)
-                        def _():
-                            each(z_down(u, k), "start")
+                    relay(u, k, sign)
                     each(x_copy(u, k), "start")
                     each(y_copy(u, k), "start")
 
@@ -212,30 +241,58 @@
         def _():
             reshape_up()
 
+        @pl.when(d == planes - 1)
+        def _():
+            send_own(2)
+
         for sign in (-1, 1):
             u = z + sign * (d - 1)
 
-            @pl.when((u >= 0) & (u < planes) & (d > 1))
-            def _():
-                each(x_in(u, 0), "wait_recv")
-                each(dy_copy(u), "start")
+            @pl.when(valid(u) & (d > 1))
+            def _():
+                @pl.when(by_y(u))
+                def _():
+                    each(x_in(u, 0), "wait_recv")
+                    each(dy_copy(u), "start")
+
+                @pl.when(~by_y(u))
+                def _():
+                    each(y_in(u, 0), "wait_recv")
+                    each(dx_copy(u), "start")
+        return carry
+
+    lax.fori_loop(1, planes + 1, step, 0)
+
+    def finish(d, carry):
+        for sign in (-1, 1):
+            u = z + sign * d
+
+            @pl.when(valid(u))
+            def _():
+                relay(u, 2, sign)
+        for sign in (-1, 1):
+            u = z + sign * d
+
+            @pl.when(valid(u))
+            def _():
+                each(x_in(u, 1), "wait_recv")
                 each(y_in(u, 1), "wait_recv")
-                each(dx_copy(u), "start")
-        for sign in (-1, 1):
-            u = z + sign * (d - 2)
-
-            @pl.when((u >= 0) & (u < planes) & (d > 2))
-            def _():
-                each(x_in(u, 1), "wait_recv")
-                each(y_in(u, 0), "wait_recv")
-                each(dy_in(u), "wait_recv")
-                each(dx_in(u), "wait_recv")
+
+                @pl.when(by_y(u))
+                def _():
+                    each(y_in(u, 0), "wait_recv")
+                    each(dy_in(u), "wait_recv")
+
+                @pl.when(~by_y(u))
+                def _():
+                    each(x_in(u, 0), "wait_recv")
+                    each(dx_in(u), "wait_recv")
                 a, b = block_dot(u)
                 acc[...] += a
                 acct[...] += b
         return carry
 
-    lax.fori_loop(1, planes + 2, step, 0)
+    lax.fori_loop(1, planes, finish, 0)
 
     swaps = [remote(acc.at[pl.ds(span, span)], other, acc_s.at[0], acc_r.at[0], here),
              remote(acct.at[:, pl.ds(span, span)], othert, acc_s.at[1], acc_r.at[1], here)]
@@ -252,7 +309,7 @@
         rng = pl.ds(k * half, half)
         out = [remote(spread.at[u, rng], spread.at[u, rng], g_s.at[slot, k, u], g_r.at[k, u], dev(s, zi, c))]
         if k == 0:
-            out.append(remote(spreadt.at[u], spreadt.at[u], g_s.at[slot, 2, u], g_r.at[2, u], dev(s, zi, c)))
+            out.append(remote(spreadt.at[u], spreadt.at[u], g_s.at[slot, PARTS, u], g_r.at[PARTS, u], dev(s, zi, c)))
         return out
 
     def lanes(si):
@@ -262,7 +319,7 @@
         rng = pl.ds(k * half, half)
         out = [remote(spread.at[u, rng], x_out.at[c, si, rng], f_s.at[k, u], f_r.at[k, si], where)]
         if k == 0:
-            out.append(remote(spreadt.at[u], rot_out.at[c, :, lanes(si)], f_s.at[2, u], f_r.at[2, si], where))
+            out.append(remote(spreadt.at[u], rot_out.at[c, :, lanes(si)], f_s.at[PARTS, u], f_r.at[PARTS, si], where))
         return out
 
     def p_copy(ci, si, k):
@@ -270,7 +327,7 @@
         out = [remote(x_out.at[ci, si, rng], x_out.at[ci, si, rng], p_s.at[k, si], p_r.at[k, si], here)]
         if k == 0:
             part = rot_out.at[ci, :, lanes(si)]
-            out.append(remote(part, part, p_s.at[2, si], p_r.at[2, si], here))
+            out.append(remote(part, part, p_s.at[PARTS, si], p_r.at[PARTS, si], here))
         return out
 
     own_copies = [pltpu.make_async_copy(spread.at[s], x_out.at[c, s], own_s.at[0]),
@@ -281,12 +338,12 @@
         def _():
             each(f_copy(u, k, dev(u, z, c), s), "start")
 
-        if k == 1:
+        if k == PARTS - 1:
             @pl.when(u == s)
             def _():
                 each(own_copies, "start")
 
-    for k in range(2):
+    for k in range(PARTS):
         @pl.when(has_up)
         def _():
             each(g_copy(z, k, z + 1, 0), "start")
@@ -298,7 +355,7 @@
         deliver(z, k)
 
     def g_step(d, carry):
-        for k in range(2):
+        for k in range(PARTS):
             for sign in (-1, 1):
                 u = z + sign * d
 
@@ -318,12 +375,12 @@
 
     lax.fori_loop(1, planes, g_step, 0)
     each(own_copies, "wait")
-    for k in range(2):
+    for k in range(PARTS):
         each(p_copy(c, s, k), "start")
 
     def p_step(i, carry):
         si = lax.rem(s + i, spots)
-        for k in range(2):
+        for k in range(PARTS):
             each(f_copy(0, k, here, si), "wait_recv")
             each(p_copy(c, si, k), "start")
         return carry
@@ -331,7 +388,7 @@
     lax.fori_loop(1, spots, p_step, 0)
 
     def p_drain(si, carry):
-        for k in range(2):
+        for k in range(PARTS):
             each(p_copy(1 - c, si, k), "wait_recv")
             each(p_copy(c, si, k), "wait_send")
         return carry
@@ -339,32 +396,40 @@
     lax.fori_loop(0, spots, p_drain, 0)
 
     def drain(u, carry):
+        for k in range(PARTS):
+            @pl.when(u != s)
+            def _():
+                each(f_copy(u, k, here, s), "wait_send")
+
+            @pl.when((u <= z) & has_up)
+            def _():
+                each(g_copy(u, k, z, 0), "wait_send")
+
+            @pl.when((u >= z) & has_down)
+            def _():
+                each(g_copy(u, k, z, 1), "wait_send")
+
+        for k in range(3):
+            @pl.when((u >= z) & has_down)
+            def _():
+                each(z_down(u, k), "wait_send")
+
+            @pl.when((u < z) & has_up)
+            def _():
+                each(z_up(u, k), "wait_send")
+
         for k in range(2):
-            @pl.when(u != s)
-            def _():
-                each(f_copy(u, k, here, s), "wait_send")
-
-            @pl.when((u <= z) & has_up)
-            def _():
-                each(g_copy(u, k, z, 0), "wait_send")
-
-            @pl.when((u >= z) & has_down)
-            def _():
-                each(g_copy(u, k, z, 1), "wait_send")
-                each(z_down(u, k), "wait_send")
-
-            @pl.when((u < z) & has_up)
-            def _():
-                each(z_up(u, k), "wait_send")
-
             @pl.when(u != z)
             def _():
                 each(x_copy(u, k), "wait_send")
                 each(y_copy(u, k), "wait_send")
 
-        @pl.when(u != z)
+        @pl.when((u != z) & by_y(u))
         def _():
             each(dy_copy(u), "wait_send")
+
+        @pl.when((u != z) & ~by_y(u))
+        def _():
             each(dx_copy(u), "wait_send")
         return carry
 
@@ -372,7 +437,7 @@
 
     @pl.when(has_up)
     def _():
-        for k in range(2):
+        for k in range(3):
             each(z_own(k), "wait_send")
 
 
@@ -446,13 +511,13 @@
             pltpu.VMEM((rope, span), F32),
             pltpu.VMEM((rope, span), F32),
             dma((planes,)), dma((planes,)), dma((planes + 2,)),
-            dma((3, planes)), dma((3, planes)), dma((3,)),
+            dma((4, planes)), dma((4, planes)), dma((4,)),
             dma((3, planes)), dma((3, planes)), dma((3, planes)), dma((3, planes)),
             dma((3, planes)), dma((3, planes)), dma((3, planes)), dma((3, planes)),
             dma((2,)), dma((2,)),
-            dma((2, 3, planes)), dma((3, planes)),
-            dma((3, planes)), dma((3, spots)),
-            dma((3, spots)), dma((3, spots)),
+            dma((2, PARTS + 1, planes)), dma((PARTS + 1, planes)),
+            dma((PARTS + 1, planes)), dma((PARTS + 1, spots)),
+            dma((PARTS + 1, spots)), dma((PARTS + 1, spots)),
             dma((4,)),
         ],
         compiler_params=pltpu.CompilerParams(collective_id=0, has_side_effects=True),

time: 55.5 us -> 55.2 us (level)
  no operation moved by 1% of the time
where the time goes in v3:
time: 55.2 us; the launch traced here: 55 us
  Pallas kernels  54.4 us (99%)
  between operations  0.64 us (1%)
    pallas_call x1, Pallas kernels, body(): pl.pallas_call(functools.partial(move_kernel, planes, spots), out_shape=(...  49.7 us
    pallas_call x1, Pallas kernels, body(): pl.pallas_call(read_kernel, grid=(CORES,), out_shape=(jax.ShapeDtypeStruc...  4.65 us

profile of v3, /device:TPU:7, one launch (start us, length us, event | category | flops | bytes accessed | tf_op | source)
XLA Modules:
  0.0 55.0 jit_solution(3657938473501381711)
XLA Ops:
  0.6 49.7 %shard_map.138 = (bf16[2,4,128,512]{3,2,1,0:T(8,128)(2,1)}, bf16[2,64,512]{2,1,0:T(8,128)(2,1)}, bf16[512,1024]{1,0:T(8,128)(2,1)}) custom-call(bf16[1,128,4096]{2,1,0:T(8,128)(2,1)} %tok.1, bf16[512,512]{1,0:T(8,128)(2,1)} %wl.1, bf16[64,512]{1,0:T(8,128)(2,1)} %bitcast.7, f32[1,512]{1,0:T(1,128)} %bitcast.8, f32[64,512]{1,0:T(8,128)} %constant.8.clone.cos_hbm, ...), custom_call_target="tpu_custom_call" | custom-call | tf_op jit(solution)/shard_map/pallas_call | solution.py:492
  50.4 4.7 %shard_map.139 = (bf16[2,2048,128]{2,1,0:T(8,128)(2,1)}, bf16[2,2048,128]{2,1,0:T(8,128)(2,1)}, bf16[2,64,512]{2,1,0:T(8,128)(2,1)}, bf16[2,4,128]{2,1,0:T(4,128)(2,1)}) custom-call(bf16[2,512,512]{2,1,0:T(8,128)(2,1)} %bitcast.6, bf16[2,64,512]{2,1,0:T(8,128)(2,1)} %get-tuple-element.12.r_ref, bf16[512,1024]{1,0:T(8,128)(2,1)} %get-tuple-element.13.up_ref, ...), custom_call_target="tpu_custom_call" | custom-call | tf_op jit(solution)/shard_map/pallas_call | solution.py:535

commit v4 on v3

--- a/solution.py
+++ b/solution.py
@@ -30,7 +30,7 @@
 
 
 def move_kernel(planes, spots, tok, wl, wr, scale, cos_hbm, sin_hbm, kup, vup, x_out, rot_out, up_out,
-                tokens, wlat, wrope, acc, acct, other, othert, spread, spreadt, kbuf, vbuf, cos_ref, sin_ref,
+                tokens, wlat, wrope, acc, acct, other, othert, spread, spreadt, kbuf, vbuf, upbuf, cos_ref, sin_ref,
                 tok_s, tok_r, own_s, z_s, z_r, zo_s, x_s, x_r, y_s, y_r, dx_s, dx_r, dy_s, dy_r,
                 acc_s, acc_r, g_s, g_r, f_s, f_r, p_s, p_r, up_s):
     s = lax.axis_index("sp")
@@ -183,25 +183,29 @@
         return (jnp.dot(x, wlat[u], preferred_element_type=F32),
                 lax.dot_general(wrope[u], x, contract, preferred_element_type=F32))
 
-    for u in range(planes):
-        own_tok(u).wait()
-        part_tok(u).wait()
-    a, b = block_dot(z)
-    acc[...] = a
-    acct[...] = b
-    get_k.wait()
-    get_v.wait()
-    get_c.wait()
-    get_n.wait()
+    def own_block():
+        for u in range(planes):
+            own_tok(u).wait()
+            part_tok(u).wait()
+        a, b = block_dot(z)
+        acc[...] = a
+        acct[...] = b
+
+    put_up = pltpu.make_async_copy(upbuf, up_out, up_s.at[4])
 
     def reshape_up():
+        get_k.wait()
+        get_v.wait()
+        get_c.wait()
+        get_n.wait()
         heads, kw = kbuf.shape[1:]
         vw = vbuf.shape[2]
         k = kbuf[...].astype(F32)
         v = vbuf[...].astype(F32)
         for h in range(heads):
-            up_out[:, h * kw:(h + 1) * kw] = k[:, h, :].astype(BF16)
-            up_out[:, heads * kw + h * vw:heads * kw + (h + 1) * vw] = v[:, h, :].astype(BF16)
+            upbuf[:, h * kw:(h + 1) * kw] = k[:, h, :].astype(BF16)
+            upbuf[:, heads * kw + h * vw:heads * kw + (h + 1) * vw] = v[:, h, :].astype(BF16)
+        put_up.start()
 
     def relay(u, k, sign):
         each(z_in(u, k), "wait_recv")
@@ -238,6 +242,10 @@
                     each(y_copy(u, k), "start")
 
         @pl.when(d == 1)
+        def _():
+            own_block()
+
+        @pl.when(d == 2)
         def _():
             reshape_up()
 
@@ -434,6 +442,7 @@
         return carry
 
     lax.fori_loop(0, planes, drain, 0)
+    put_up.wait()
 
     @pl.when(has_up)
     def _():
@@ -495,7 +504,7 @@
                    jax.ShapeDtypeStruct((CORES, rope, length), BF16),
                    jax.ShapeDtypeStruct((lat, heads * (kw + vw)), BF16)),
         in_specs=[hbm, hbm, hbm, vmem, hbm, hbm, hbm, hbm],
-        out_specs=(vmem, vmem, vmem),
+        out_specs=(vmem, vmem, hbm),
         scratch_shapes=[
             pltpu.VMEM((CORES, planes, span, rows), BF16),
             pltpu.VMEM((planes, rows, lat), BF16),
@@ -508,6 +517,7 @@
             pltpu.VMEM((planes, rope, span), BF16),
             pltpu.VMEM(key_up.shape, BF16),
             pltpu.VMEM(value_up.shape, BF16),
+            pltpu.VMEM((lat, heads * (kw + vw)), BF16),
             pltpu.VMEM((rope, span), F32),
             pltpu.VMEM((rope, span), F32),
             dma((planes,)), dma((planes,)), dma((planes + 2,)),
@@ -518,7 +528,7 @@
             dma((2, PARTS + 1, planes)), dma((PARTS + 1, planes)),
             dma((PARTS + 1, planes)), dma((PARTS + 1, spots)),
             dma((PARTS + 1, spots)), dma((PARTS + 1, spots)),
-            dma((4,)),
+            dma((5,)),
         ],
         compiler_params=pltpu.CompilerParams(collective_id=0, has_side_effects=True),
     )(tokens, latent_down, rope_weight.T, norm_scale.reshape(1, lat),

time: 55.2 us -> 55.1 us (level)
  no operation moved by 1% of the time
where the time goes in v4:
time: 55.1 us; the launch traced here: 54.9 us
  Pallas kernels  54.3 us (99%)
  between operations  0.64 us (1%)
    pallas_call x1, Pallas kernels, body(): pl.pallas_call(functools.partial(move_kernel, planes, spots), out_shape=(...  49.6 us
    pallas_call x1, Pallas kernels, body(): pl.pallas_call(read_kernel, grid=(CORES,), out_shape=(jax.ShapeDtypeStruc...  4.65 us

profile of v4, /device:TPU:7, one launch (start us, length us, event | category | flops | bytes accessed | tf_op | source)
XLA Modules:
  0.0 54.9 jit_solution(16629430815330101684)
XLA Ops:
  0.6 49.6 %shard_map.138 = (bf16[2,4,128,512]{3,2,1,0:T(8,128)(2,1)}, bf16[2,64,512]{2,1,0:T(8,128)(2,1)}, bf16[512,1024]{1,0:T(8,128)(2,1)}) custom-call(bf16[1,128,4096]{2,1,0:T(8,128)(2,1)} %tok.1, bf16[512,512]{1,0:T(8,128)(2,1)} %wl.1, bf16[64,512]{1,0:T(8,128)(2,1)} %bitcast.7, f32[1,512]{1,0:T(1,128)} %bitcast.8, f32[64,512]{1,0:T(8,128)} %constant.8.clone.cos_hbm, ...), custom_call_target="tpu_custom_call" | custom-call | tf_op jit(solution)/shard_map/pallas_call | solution.py:501
  50.3 4.7 %shard_map.139 = (bf16[2,2048,128]{2,1,0:T(8,128)(2,1)}, bf16[2,2048,128]{2,1,0:T(8,128)(2,1)}, bf16[2,64,512]{2,1,0:T(8,128)(2,1)}, bf16[2,4,128]{2,1,0:T(4,128)(2,1)}) custom-call(bf16[2,512,512]{2,1,0:T(8,128)(2,1)} %bitcast.6, bf16[2,64,512]{2,1,0:T(8,128)(2,1)} %get-tuple-element.12.r_ref, bf16[512,1024]{1,0:T(8,128)(2,1)} %get-tuple-element.13.up_ref, ...), custom_call_target="tpu_custom_call" | custom-call | tf_op jit(solution)/shard_map/pallas_call | solution.py:545

commit v5 on v4

--- a/solution.py
+++ b/solution.py
@@ -386,14 +386,14 @@
     for k in range(PARTS):
         each(p_copy(c, s, k), "start")
 
-    def p_step(i, carry):
-        si = lax.rem(s + i, spots)
-        for k in range(PARTS):
+    for k in range(PARTS):
+        def p_step(i, carry):
+            si = lax.rem(s + i, spots)
             each(f_copy(0, k, here, si), "wait_recv")
             each(p_copy(c, si, k), "start")
-        return carry
-
-    lax.fori_loop(1, spots, p_step, 0)
+            return carry
+
+        lax.fori_loop(1, spots, p_step, 0)
 
     def p_drain(si, carry):
         for k in range(PARTS):

time: 55.1 us -> 54.9 us (level)
  no operation moved by 1% of the time
where the time goes in v5:
time: 54.9 us; the launch traced here: 54.8 us
  Pallas kernels  54.1 us (99%)
  between operations  0.64 us (1%)
    pallas_call x1, Pallas kernels, body(): pl.pallas_call(functools.partial(move_kernel, planes, spots), out_shape=(...  49.5 us
    pallas_call x1, Pallas kernels, body(): pl.pallas_call(read_kernel, grid=(CORES,), out_shape=(jax.ShapeDtypeStruc...  4.65 us

profile of v5, /device:TPU:7, one launch (start us, length us, event | category | flops | bytes accessed | tf_op | source)
XLA Modules:
  0.0 54.8 jit_solution(1030915042310033166)
XLA Ops:
  0.6 49.5 %shard_map.138 = (bf16[2,4,128,512]{3,2,1,0:T(8,128)(2,1)}, bf16[2,64,512]{2,1,0:T(8,128)(2,1)}, bf16[512,1024]{1,0:T(8,128)(2,1)}) custom-call(bf16[1,128,4096]{2,1,0:T(8,128)(2,1)} %tok.1, bf16[512,512]{1,0:T(8,128)(2,1)} %wl.1, bf16[64,512]{1,0:T(8,128)(2,1)} %bitcast.7, f32[1,512]{1,0:T(1,128)} %bitcast.8, f32[64,512]{1,0:T(8,128)} %constant.8.clone.cos_hbm, ...), custom_call_target="tpu_custom_call" | custom-call | tf_op jit(solution)/shard_map/pallas_call | solution.py:501
  50.1 4.7 %shard_map.139 = (bf16[2,2048,128]{2,1,0:T(8,128)(2,1)}, bf16[2,2048,128]{2,1,0:T(8,128)(2,1)}, bf16[2,64,512]{2,1,0:T(8,128)(2,1)}, bf16[2,4,128]{2,1,0:T(4,128)(2,1)}) custom-call(bf16[2,512,512]{2,1,0:T(8,128)(2,1)} %bitcast.6, bf16[2,64,512]{2,1,0:T(8,128)(2,1)} %get-tuple-element.12.r_ref, bf16[512,1024]{1,0:T(8,128)(2,1)} %get-tuple-element.13.up_ref, ...), custom_call_target="tpu_custom_call" | custom-call | tf_op jit(solution)/shard_map/pallas_call | solution.py:545
